TPU v7x, 512 devices: a whole 4x8x8 slice. The times are simulated.
512 devices in a mesh: sp: 128 (over z, y, core), tp: 4 (over x).
Axes of the slice: x: 4, y: 8, z: 8, core: 2. Of those that a mesh axis runs over, the one named last changes fastest.
Arguments:
- tokens: bfloat16 [32768, 2048], P(('sp', 'tp')), may hold values from -16 to 16
- w_query: bfloat16 [2048, 1024], P(None, 'tp'), may hold values from -1 to 1
- w_key: bfloat16 [2048, 256], P(None, 'tp'), may hold values from -1 to 1
- w_value: bfloat16 [2048, 256], P(None, 'tp'), may hold values from -0.125 to 0.125
- w_gate: bfloat16 [2048, 16], P(None, 'tp'), may hold values from -0.125 to 0.125
- gate_bias: float32 [16], P('tp'), as said below
- w_output: bfloat16 [1024, 2048], P('tp'), may hold values from -0.1875 to 0.1875
Outputs:
- mixed: bfloat16 [32768, 2048], P(('sp', 'tp'))
Inputs may be any that keep to these rules, and one draw needn't show every extreme that they name: `gate_bias`: each head's forget gate bias is 4 or more; there is no upper bound.
All inputs are finite; a program needn't handle non-finite values.
Results may differ from a plain program's by a relative error of at most 0.012.
The roundings to bfloat16 on the way count: a program that leaves them out, or rounds other values in their place, can miss the bound.
Values may be sent and summed in bfloat16 or wider, within the bound.
A program may use at most 64 MiB of HBM per device.

v0:
```python
import functools

import jax
import jax.numpy as jnp
from jax import lax
from jax.experimental import pallas as pl
from jax.experimental.pallas import tpu as pltpu
from jax.sharding import PartitionSpec as P

HEAD = 64
LANES = 128
masked_value = -1e30
MESH = pl.DeviceIdType.MESH


def kernel(
    sp, tp, chunks, out_chunks,
    tokens, w_query, w_key, w_value, w_gate, bias_in, w_output,
    out,
    tok, w_all, w_kv, w_g, wo, wo_pair, proj, logits, qs, kv, cum, own_sum, pair_sum,
    peak, mass, accum, att, att_pair, keep, outgoing, incoming, bias,
    local_sem, own_sem, cross_send, cross_recv, pair_send, pair_recv, relay_send, relay_recv,
    wo_send, wo_recv, kv_send, kv_recv, cum_send, cum_recv,
    kv_side, cum_side, sum_send, sum_recv,
    att_send, att_recv, out_send, out_recv,
):
    lo_n = 2
    hi_n = tp // lo_n
    me = lax.axis_index("sp")
    t_me = lax.axis_index("tp")
    hi, lo = lax.div(t_me, lo_n), lax.rem(t_me, lo_n)
    pair = hi * lo_n + (1 - lo)
    rows = tok.shape[1]
    local_rows = rows * tp
    width = tok.shape[2]
    q_cols = w_query.shape[1]
    heads = w_gate.shape[0]
    key_cols = w_key.shape[0]
    span_n = 2
    far_n = sp // span_n
    far, side = lax.div(me, span_n), lax.rem(me, span_n)
    mate = far * span_n + (1 - side)
    piece = width // chunks
    out_cols = w_output.shape[1]
    out_piece = out_cols // out_chunks
    group = lo_n * rows
    half = 4

    def cross(d):
        return lax.rem(hi + d, hi_n) * lo_n + lo

    loads = [
        pltpu.make_async_copy(w_key, w_kv.at[pl.ds(0, key_cols)], local_sem.at[0]),
        pltpu.make_async_copy(w_value, w_kv.at[pl.ds(key_cols, key_cols)], local_sem.at[1]),
        pltpu.make_async_copy(w_gate, w_g, local_sem.at[2]),
        pltpu.make_async_copy(w_query, w_all.at[:, pl.ds(0, q_cols)], local_sem.at[3]),
        pltpu.make_async_copy(w_output, wo, local_sem.at[4]),
        pltpu.make_async_copy(bias_in, bias, local_sem.at[5]),
    ]
    own = pltpu.make_async_copy(tokens, tok.at[t_me], own_sem)
    own.start()
    for load in loads:
        load.start()

    barrier = pltpu.get_barrier_semaphore()
    pl.semaphore_signal(barrier, inc=1, device_id={"tp": pair}, device_id_type=MESH)
    for d in range(1, hi_n):
        pl.semaphore_signal(barrier, inc=1, device_id={"tp": cross(d)}, device_id_type=MESH)

    def greet(d, carry):
        other = lax.rem(far + d, far_n) * span_n + side
        pl.semaphore_signal(barrier, inc=1, device_id={"sp": other}, device_id_type=MESH)
        return carry

    lax.fori_loop(1, far_n, greet, 0)
    pl.semaphore_signal(barrier, inc=1, device_id={"sp": mate}, device_id_type=MESH)
    pl.semaphore_wait(barrier, 1 + (hi_n - 1) + (far_n - 1) + 1)

    def cols(k):
        return pl.ds(k * piece, piece)

    def cross_copy(d, k):
        return pltpu.make_async_remote_copy(
            tok.at[t_me, :, cols(k)], tok.at[t_me, :, cols(k)],
            cross_send.at[d - 1, k], cross_recv.at[d - 1, k],
            device_id={"tp": cross(d)}, device_id_type=MESH,
        )

    def pair_copy(k):
        return pltpu.make_async_remote_copy(
            tok.at[t_me, :, cols(k)], tok.at[t_me, :, cols(k)],
            pair_send.at[k], pair_recv.at[k],
            device_id={"tp": pair}, device_id_type=MESH,
        )

    def relay_copy(d, k):
        source = lax.rem(hi - d + hi_n, hi_n) * lo_n + lo
        return pltpu.make_async_remote_copy(
            tok.at[source, :, cols(k)], tok.at[source, :, cols(k)],
            relay_send.at[d - 1, k], relay_recv.at[d - 1, k],
            device_id={"tp": pair}, device_id_type=MESH,
        )

    own.wait()
    for k in range(chunks):
        for d in range(1, hi_n):
            cross_copy(d, k).start()
    for k in range(chunks):
        pair_copy(k).start()

    for load in loads[:3]:
        load.wait()
    build = 256

    def assemble(i, carry):
        span = pl.ds(pl.multiple_of(i * build, build), build)
        w_all[span, q_cols:] = w_kv[:, span].T
        return carry

    lax.fori_loop(0, width // build, assemble, 0)
    loads[3].wait()
    loads[4].wait()
    loads[5].wait()
    wo_copy = pltpu.make_async_remote_copy(
        wo, wo_pair, wo_send, wo_recv, device_id={"tp": pair}, device_id_type=MESH
    )

    for k in range(chunks):
        for d in range(1, hi_n):
            cross_copy(d, k).wait_recv()
            relay_copy(d, k).start()
        pair_copy(k).wait_recv()
        for d in range(1, hi_n):
            relay_copy(d, k).wait_recv()
        here = tok[:, :, k * piece:(k + 1) * piece].reshape(local_rows, piece)
        part = jnp.dot(here, w_all[k * piece:(k + 1) * piece, :], preferred_element_type=jnp.float32)
        gate_part = lax.dot_general(
            w_g[:, k * piece:(k + 1) * piece], here, (((1,), (1,)), ((), ())),
            preferred_element_type=jnp.float32,
        )
        if k == 0:
            proj[...] = part
            logits[0:heads, :] = gate_part
        else:
            proj[...] += part
            logits[0:heads, :] += gate_part
    wo_copy.start()

    row_of = lax.broadcasted_iota(jnp.int32, (8, local_rows), 0)
    u = jnp.where(row_of < heads, logits[...].astype(jnp.bfloat16).astype(jnp.float32), 0.0)
    for h in range(heads):
        u = jnp.where(row_of == h, u + bias[h], u)
    gates = jnp.minimum(u, 0.0) - jnp.log1p(jnp.exp(-jnp.abs(u)))
    upper = (
        lax.broadcasted_iota(jnp.int32, (local_rows, local_rows), 0)
        <= lax.broadcasted_iota(jnp.int32, (local_rows, local_rows), 1)
    )
    ones = jnp.where(upper, 1.0, 0.0).astype(jnp.bfloat16)
    g0 = gates.astype(jnp.bfloat16)
    r1 = gates - g0.astype(jnp.float32)
    g1 = r1.astype(jnp.bfloat16)
    g2 = (r1 - g1.astype(jnp.float32)).astype(jnp.bfloat16)
    total = jnp.dot(g2, ones, preferred_element_type=jnp.float32)
    total = total + jnp.dot(g1, ones, preferred_element_type=jnp.float32)
    total = total + jnp.dot(g0, ones, preferred_element_type=jnp.float32)
    own_sum[...] = jnp.broadcast_to(total[:, local_rows - 1:], (8, LANES))
    sum_copy = pltpu.make_async_remote_copy(
        own_sum, pair_sum, sum_send, sum_recv, device_id={"sp": mate}, device_id_type=MESH
    )
    sum_copy.start()

    kv[me] = proj[:, q_cols:q_cols + 2 * key_cols].astype(jnp.bfloat16)
    scale = HEAD ** -0.5
    for h in range(heads):
        q = proj[:, h * HEAD:(h + 1) * HEAD].astype(jnp.bfloat16) * jnp.bfloat16(scale)
        q = jnp.concatenate([q, jnp.zeros((local_rows, LANES - HEAD), jnp.bfloat16)], axis=1)
        for g in range(hi_n):
            qs[g, h * group:(h + 1) * group, :] = q[g * group:(g + 1) * group]

    def column(d):
        return (
            pltpu.make_async_remote_copy(
                kv.at[me], kv.at[me], kv_send.at[d], kv_recv.at[me],
                device_id={"sp": d * span_n + side}, device_id_type=MESH,
            ),
            pltpu.make_async_remote_copy(
                cum.at[me], cum.at[me], cum_send.at[d], cum_recv.at[me],
                device_id={"sp": d * span_n + side}, device_id_type=MESH,
            ),
        )

    def across(r):
        return (
            pltpu.make_async_remote_copy(
                kv.at[r], kv.at[r], kv_side.at[lax.div(r, span_n)], kv_recv.at[r],
                device_id={"sp": mate}, device_id_type=MESH,
            ),
            pltpu.make_async_remote_copy(
                cum.at[r], cum.at[r], cum_side.at[lax.div(r, span_n)], cum_recv.at[r],
                device_id={"sp": mate}, device_id_type=MESH,
            ),
        )

    later = far_n - 1 - far

    def send_column(which, i, carry):
        column(far + 1 + i)[which].start()
        return carry

    lax.fori_loop(0, jnp.minimum(later, 1), functools.partial(send_column, 0), 0)

    @pl.when(side == 0)
    def _():
        across(me)[0].start()

    halves = local_rows // LANES

    def lane_parts(x):
        return [x[:, j * LANES:(j + 1) * LANES] for j in range(halves)]

    def attend(g, kv_here, shift, first):
        s = lax.dot_general(
            qs[g], kv_here, (((1,), (1,)), ((), ())), preferred_element_type=jnp.float32
        )
        weights = []
        rescales = []
        for h in range(heads):
            here = slice(h * group, (h + 1) * group)
            x = s[here] + shift[h:h + 1, :]
            if first:
                allowed = (
                    lax.broadcasted_iota(jnp.int32, (group, local_rows), 1)
                    <= lax.broadcasted_iota(jnp.int32, (group, local_rows), 0) + g * group
                )
                x = jnp.where(allowed, x, masked_value)
            top = jnp.max(x, axis=1, keepdims=True)
            if first:
                new_peak = jnp.broadcast_to(top, (group, LANES))
            else:
                old_peak = peak[here, :]
                new_peak = jnp.maximum(old_peak, top)
                rescale = jnp.exp(old_peak - new_peak)
                rescales.append(rescale)
            p = [jnp.exp(part - new_peak) for part in lane_parts(x)]
            p_sum = functools.reduce(lambda a, b: a + b, p)
            weights.append(jnp.concatenate([part.astype(jnp.bfloat16) for part in p], axis=1))
            peak[here, :] = new_peak
            mass[here, :] = p_sum if first else mass[here, :] * rescale + p_sum
        term = jnp.dot(
            jnp.concatenate(weights, axis=0), kv_here, preferred_element_type=jnp.float32
        )
        for h in range(heads):
            here = slice(h * group, (h + 1) * group)
            if first:
                accum[here, :] = term[here]
            else:
                accum[here, :] = accum[here, :] * rescales[h] + term[here]

    def pass_over(g, fresh):
        attend(g, kv[me], -total, True)
        if fresh:
            sum_copy.wait_recv()
            start = jnp.where(side == 1, pair_sum[:, :1], 0.0)
            both_sums = jnp.broadcast_to((own_sum[...] + pair_sum[...])[:, :1], (8, local_rows))
            cum[me] = jnp.concatenate([(total + start)[:half], both_sums[:half]], axis=0)
            lax.fori_loop(0, later, functools.partial(send_column, 1), 0)
            lax.fori_loop(1, later, functools.partial(send_column, 0), 0)

            @pl.when(side == 0)
            def _():
                across(me)[1].start()

        start = jnp.where(side == 1, pair_sum[0:half, :1], 0.0)

        def same_side(i, base):
            r = (far - 1 - i) * span_n + side
            if fresh:
                for copy in across(r):
                    copy.wait_recv()
                for copy in across(r):
                    copy.start()
            base = base + cum[r, half:, 0:1]
            attend(g, kv[r], base - cum[r, 0:half, :], False)
            return base

        lax.fori_loop(0, far, same_side, start)

        @pl.when(side == 1)
        def _():
            if fresh:
                for copy in across(mate):
                    copy.wait_recv()
            attend(g, kv[mate], start - cum[mate, 0:half, :], False)

        def other_side(i, base):
            r = (far - 1 - i) * span_n + 1 - side
            if fresh:
                for copy in across(r):
                    copy.wait_recv()
            base = base + cum[r, half:, 0:1]
            attend(g, kv[r], base - cum[r, 0:half, :], False)
            return base

        lax.fori_loop(0, far, other_side, start)

        for h in range(heads):
            here = slice(h * group, (h + 1) * group)
            denominator = jnp.sum(mass[here, :], axis=1, keepdims=True)
            done = (accum[here, key_cols:2 * key_cols] / denominator).astype(jnp.bfloat16)
            att[g, :, :, h * HEAD:(h + 1) * HEAD] = done.reshape(lo_n, rows, HEAD)

    def att_copy(g):
        return pltpu.make_async_remote_copy(
            att.at[g, 1 - lo], att_pair.at[g], att_send.at[g], att_recv.at[g],
            device_id={"tp": pair}, device_id_type=MESH,
        )

    def out_copy(d, k):
        span = pl.ds(k * out_piece, out_piece)
        return pltpu.make_async_remote_copy(
            outgoing.at[d - 1, :, span], incoming.at[d - 1, :, span],
            out_send.at[d - 1, k], out_recv.at[d - 1, k],
            device_id={"tp": cross(d)}, device_id_type=MESH,
        )

    def combined(g, k):
        span = slice(k * out_piece, (k + 1) * out_piece)
        a = jnp.dot(att[g, lo], wo[:, span], preferred_element_type=jnp.float32)
        b = jnp.dot(att_pair[g], wo_pair[:, span], preferred_element_type=jnp.float32)
        return (
            a.astype(jnp.bfloat16).astype(jnp.float32) + b.astype(jnp.bfloat16).astype(jnp.float32)
        )

    for d in list(range(1, hi_n)):
        g = lax.rem(hi + d, hi_n)
        pass_over(g, d == 1)
        att_copy(g).start()
        if d == 1:
            wo_copy.wait_recv()
        att_copy(g).wait_recv()
        for k in range(out_chunks):
            span = slice(k * out_piece, (k + 1) * out_piece)
            outgoing[d - 1, :, span] = combined(g, k).astype(jnp.bfloat16)
            out_copy(d, k).start()
    pass_over(hi, False)
    att_copy(hi).start()
    att_copy(hi).wait_recv()
    for k in range(out_chunks):
        keep[:, k * out_piece:(k + 1) * out_piece] = combined(hi, k)
    for k in range(out_chunks):
        span = slice(k * out_piece, (k + 1) * out_piece)
        value = keep[:, span]
        for d in range(1, hi_n):
            out_copy(d, k).wait_recv()
            value = value + incoming[d - 1, :, span].astype(jnp.float32)
        out[:, span] = value.astype(jnp.bfloat16)

    for k in range(chunks):
        for d in range(1, hi_n):
            cross_copy(d, k).wait_send()
            relay_copy(d, k).wait_send()
        pair_copy(k).wait_send()
    wo_copy.wait_send()
    for d in range(hi_n):
        att_copy(d).wait_send()
    for k in range(out_chunks):
        for d in range(1, hi_n):
            out_copy(d, k).wait_send()

    sum_copy.wait_send()

    @pl.when(side == 0)
    def _():
        for copy in across(me):
            copy.wait_send()

    def drain(i, carry):
        for copy in column(far_n - 1 - i):
            copy.wait_send()
        return carry

    lax.fori_loop(0, later, drain, 0)

    def drain_side(i, carry):
        for copy in across((far - 1 - i) * span_n + side):
            copy.wait_send()
        return carry

    lax.fori_loop(0, far, drain_side, 0)


def shards(tokens, w_query, w_key, w_value, w_gate, gate_bias, w_output):
    sp = lax.axis_size("sp")
    tp = lax.axis_size("tp")
    rows, width = tokens.shape
    local_rows = rows * tp
    q_cols, key_cols, heads = w_query.shape[1], w_key.shape[1], w_gate.shape[1]
    out_cols = w_output.shape[1]
    assert tp % 2 == 0 and sp % 2 == 0 and tp >= 4 and 2 * key_cols == LANES and key_cols == HEAD and heads <= 4
    hi_n = tp // 2
    chunks = 2
    out_chunks = 2
    bf, f32 = jnp.bfloat16, jnp.float32
    dma = pltpu.SemaphoreType.DMA
    hbm_spec = pl.BlockSpec(memory_space=pltpu.HBM)
    vmem_spec = pl.BlockSpec(memory_space=pltpu.VMEM)
    operands = (tokens, w_query, w_key.T, w_value.T, w_gate.T, gate_bias, w_output)
    return pl.pallas_call(
        functools.partial(kernel, sp, tp, chunks, out_chunks),
        out_shape=jax.ShapeDtypeStruct((rows, out_cols), bf),
        in_specs=[hbm_spec] * 7,
        out_specs=vmem_spec,
        scratch_shapes=[
            pltpu.VMEM((tp, rows, width), bf),
            pltpu.VMEM((width, q_cols + LANES), bf),
            pltpu.VMEM((LANES, width), bf),
            pltpu.VMEM((heads, width), bf),
            pltpu.VMEM(w_output.shape, bf),
            pltpu.VMEM(w_output.shape, bf),
            pltpu.VMEM((local_rows, q_cols + LANES), f32),
            pltpu.VMEM((8, local_rows), f32),
            pltpu.VMEM((hi_n, heads * 2 * rows, LANES), bf),
            pltpu.VMEM((sp, local_rows, LANES), bf),
            pltpu.VMEM((sp, 8, local_rows), f32),
            pltpu.VMEM((8, LANES), f32),
            pltpu.VMEM((8, LANES), f32),
            pltpu.VMEM((heads * 2 * rows, LANES), f32),
            pltpu.VMEM((heads * 2 * rows, LANES), f32),
            pltpu.VMEM((heads * 2 * rows, LANES), f32),
            pltpu.VMEM((hi_n, 2, rows, q_cols), bf),
            pltpu.VMEM((hi_n, rows, q_cols), bf),
            pltpu.VMEM((rows, out_cols), f32),
            pltpu.VMEM((hi_n - 1, rows, out_cols), bf),
            pltpu.VMEM((max(hi_n - 1, 1), rows, out_cols), bf),
            pltpu.SMEM((heads,), f32),
            dma((6,)),
            dma,
            dma((hi_n - 1, chunks)),
            dma((hi_n - 1, chunks)),
            dma((chunks,)),
            dma((chunks,)),
            dma((hi_n - 1, chunks)),
            dma((hi_n - 1, chunks)),
            dma,
            dma,
            dma((sp // 2,)),
            dma((sp,)),
            dma((sp // 2,)),
            dma((sp,)),
            dma((sp // 2,)),
            dma((sp // 2,)),
            dma,
            dma,
            dma((hi_n,)),
            dma((hi_n,)),
            dma((hi_n - 1, out_chunks)),
            dma((hi_n - 1, out_chunks)),
        ],
        compiler_params=pltpu.CompilerParams(
            collective_id=0, has_side_effects=True, vmem_limit_bytes=(20 << 20) + (sp << 17)
        ),
    )(*(pltpu.with_memory_space_constraint(x, pltpu.HBM) for x in operands))


def solution(mesh):
    return jax.shard_map(
        shards,
        mesh=mesh,
        in_specs=(
            P(("sp", "tp"), None),
            P(None, "tp"),
            P(None, "tp"),
            P(None, "tp"),
            P(None, "tp"),
            P("tp"),
            P("tp", None),
        ),
        out_specs=P(("sp", "tp"), None),
        check_vma=False,
    )
```

profile of v0, /device:TPU:505, one launch (start us, length us, event | category | flops | bytes accessed | tf_op | source)
XLA Modules:
  0.0 295.9 jit_solution(7666534555424701455)
XLA Ops:
  0.0 295.1 %shard_map.73 = bf16[64,2048]{1,0:T(8,128)(2,1)S(1)} custom-call(bf16[64,2048]{1,0:T(8,128)(2,1)} %tokens.1, bf16[2048,256]{1,0:T(8,128)(2,1)} %w_query.1, bf16[64,2048]{1,0:T(8,128)(2,1)} %bitcast.3, bf16[64,2048]{1,0:T(8,128)(2,1)} %bitcast.4, bf16[4,2048]{1,0:T(4,128)(2,1)} %bitcast.5, f32[4]{0:T(128)} %bias_in.1, bf16[256,2048]{1,0:T(8,128)(2,1)} %w_output.1), custom_call_target="tpu_custom_call" | custom-call | tf_op jit(solution)/shard_map/pallas_call | solution.py:408
  295.2 0.7 copy.9
where the time goes:
time: 296 us
  Pallas kernels  295 us (100%)
    pallas_call x1, Pallas kernels, shards(): pl.pallas_call(functools.partial(kernel, sp, tp, chunks, out_chunks), out...  295 us

commit v1 on v0

v1 whole, which is shorter than its diff:
```python
import functools

import jax
import jax.numpy as jnp
from jax import lax
from jax.experimental import pallas as pl
from jax.experimental.pallas import tpu as pltpu
from jax.sharding import PartitionSpec as P

HEAD = 64
LANES = 128
AUG = 16
RING = 8
masked_value = -1e30
skipped_value = -1e38
MESH = pl.DeviceIdType.MESH
f32, bf = jnp.float32, jnp.bfloat16


def pieces_of(x):
    a = x.astype(bf)
    r = x - a.astype(f32)
    b = r.astype(bf)
    c = (r - b.astype(f32)).astype(bf)
    return a, b, c


def kernel(
    sp, tp, ny, chunks,
    tokens, w_query, w_key, w_value, w_gate, bias_in, w_output,
    out,
    tok, wq_raw, wt, w_g, wo_all, proj, kx, qa, own_sum, pair_sum, sums, gk, gq,
    score, weight, tile_max, scaling, peak, acc, x_in, ret_o, ret_s, in_o, in_s,
    att_t, att_out, att_all, bias,
    local_sem, own_sem, ta_send, ta_recv, tb_send, tb_recv,
    sum_send, sum_recv, tot_send, tot_recv,
    q_send, q_recv, pq_send, pq_recv, fq_send, fq_recv,
    z_send, a_send, b_send, kx_recv,
    wa_send, wa_recv, wb_send, wb_recv, wm_send, wm_recv,
    x_send, x_recv, r_send, r_recv, att_send, att_recv,
):
    me = lax.axis_index("sp")
    x = lax.axis_index("tp")
    far_n = sp // 2
    nz = far_n // ny
    deep = nz // 2
    far, side = lax.div(me, 2), lax.rem(me, 2)
    z, y = lax.div(far, ny), lax.rem(far, ny)
    mate = far * 2 + (1 - side)
    sign = 1 - 2 * side
    rows = tok.shape[1]
    local_rows = rows * tp
    width = tok.shape[2]
    q_cols = w_query.shape[1]
    heads = w_gate.shape[0]
    key_cols = w_key.shape[0]
    piece = width // chunks
    kv_at = q_cols
    gate_at = q_cols + 2 * key_cols
    ka_rows = key_cols + AUG
    lanes = heads * local_rows
    out_cols = w_output.shape[1]
    a_hops, b_hops = ny // 2, ny // 2 - 1
    xa_hops, xb_hops = tp // 2, tp // 2 - 1
    heavy = z >= deep
    other_z = nz - 1 - z
    partner_far = other_z * ny + y
    partner = partner_far * 2 + side
    x_a = lax.rem(x + sign + tp, tp)
    x_b = lax.rem(x - sign + tp, tp)
    y_a = (z * ny + lax.rem(y + sign + ny, ny)) * 2 + side
    y_b = (z * ny + lax.rem(y - sign + ny, ny)) * 2 + side

    loads = [
        pltpu.make_async_copy(w_query, wq_raw, local_sem.at[0]),
        pltpu.make_async_copy(w_key, wt.at[pl.ds(kv_at, key_cols)], local_sem.at[1]),
        pltpu.make_async_copy(w_value, wt.at[pl.ds(kv_at + key_cols, key_cols)], local_sem.at[2]),
        pltpu.make_async_copy(w_gate, w_g, local_sem.at[3]),
        pltpu.make_async_copy(bias_in, bias, local_sem.at[4]),
        pltpu.make_async_copy(w_output.at[pl.ds(0, q_cols // 2)], wo_all.at[x, 0], local_sem.at[5]),
        pltpu.make_async_copy(w_output.at[pl.ds(q_cols // 2, q_cols // 2)], wo_all.at[x, 1], local_sem.at[6]),
    ]
    own = pltpu.make_async_copy(tokens, tok.at[x], own_sem)
    own.start()
    for load in loads:
        load.start()

    barrier = pltpu.get_barrier_semaphore()
    for d in range(1, tp):
        pl.semaphore_signal(barrier, inc=1, device_id={"tp": lax.rem(x + d, tp)}, device_id_type=MESH)
    pl.semaphore_signal(barrier, inc=1, device_id={"sp": mate}, device_id_type=MESH)

    def greet(d, carry):
        other = lax.rem(far + d, far_n) * 2 + side
        pl.semaphore_signal(barrier, inc=1, device_id={"sp": other}, device_id_type=MESH)
        return carry

    lax.fori_loop(1, far_n, greet, 0)
    pl.semaphore_wait(barrier, (tp - 1) + 1 + (far_n - 1))

    def remote(src, dst, send, recv, axis, index):
        return pltpu.make_async_remote_copy(
            src, dst, send, recv, device_id={axis: index}, device_id_type=MESH
        )

    def tok_a(d, k):
        ref = tok.at[lax.rem(x - sign * d + tp, tp), :, pl.ds(k * piece, piece)]
        return remote(ref, ref, ta_send.at[d, k], ta_recv.at[d, k], "tp", x_a)

    def tok_b(d, k):
        ref = tok.at[lax.rem(x + sign * d + tp, tp), :, pl.ds(k * piece, piece)]
        return remote(ref, ref, tb_send.at[d, k], tb_recv.at[d, k], "tp", x_b)

    own.wait()
    for k in range(chunks):
        tok_a(0, k).start()
        if xb_hops:
            tok_b(0, k).start()

    for load in loads[:5]:
        load.wait()
    build = 256
    for i in range(width // build):
        wt[0:q_cols, i * build:(i + 1) * build] = wq_raw[i * build:(i + 1) * build, :].T
    wt[gate_at:gate_at + AUG, :] = jnp.concatenate(
        [w_g[...].astype(f32), jnp.zeros((AUG - heads, width), f32)], axis=0
    ).astype(bf)

    q_row = lax.broadcasted_iota(jnp.int32, (AUG, lanes), 0)
    q_head = lax.div(lax.broadcasted_iota(jnp.int32, (AUG, lanes), 1), local_rows)
    pattern = jnp.where(
        (q_row < 3 * heads) & (lax.rem(q_row, heads) == q_head), 1.0, 0.0
    ).astype(bf)
    for i in range(4):
        qa[i, key_cols:ka_rows, :] = pattern

    for k in range(chunks):
        for d in range(1, xa_hops + 1):
            tok_a(d - 1, k).wait_recv()
            if d < xa_hops:
                tok_a(d, k).start()
            if d <= xb_hops:
                tok_b(d - 1, k).wait_recv()
                if d < xb_hops:
                    tok_b(d, k).start()
        here = tok[:, :, k * piece:(k + 1) * piece].reshape(local_rows, piece)
        part = lax.dot_general(
            wt[:, k * piece:(k + 1) * piece], here, (((1,), (1,)), ((), ())),
            preferred_element_type=f32,
        )
        if k == 0:
            proj[...] = part
        else:
            proj[...] += part

    row_of = lax.broadcasted_iota(jnp.int32, (8, local_rows), 0)
    u = proj[gate_at:gate_at + 8, :].astype(bf).astype(f32)
    for h in range(heads):
        u = jnp.where(row_of == h, u + bias[h], u)
    gates = jnp.minimum(u, 0.0) - jnp.log1p(jnp.exp(-jnp.abs(u)))
    gates = jnp.where(row_of < heads, gates, 0.0)
    upper = (
        lax.broadcasted_iota(jnp.int32, (local_rows, local_rows), 0)
        <= lax.broadcasted_iota(jnp.int32, (local_rows, local_rows), 1)
    )
    ones = jnp.where(upper, 1.0, 0.0).astype(bf)
    g0, g1, g2 = pieces_of(gates)
    total = jnp.dot(g2, ones, preferred_element_type=f32)
    total = total + jnp.dot(g1, ones, preferred_element_type=f32)
    total = total + jnp.dot(g0, ones, preferred_element_type=f32)
    own_sum[...] = jnp.broadcast_to(total[:, local_rows - 1:], (8, LANES))
    sum_copy = remote(own_sum, pair_sum, sum_send, sum_recv, "sp", mate)
    sum_copy.start()

    s0, s1, s2 = [p.astype(f32)[:heads] for p in pieces_of(-total)]
    last = jnp.where(lax.broadcasted_iota(jnp.int32, (AUG - 3 * heads, local_rows), 0) == 0, 1.0, 0.0)
    kx[far, 0:key_cols, :] = proj[kv_at:kv_at + key_cols, :].astype(bf)
    kx[far, key_cols:ka_rows, :] = jnp.concatenate([s0, s1, s2, last], axis=0).astype(bf)
    kx[far, ka_rows:, :] = proj[kv_at + key_cols:kv_at + 2 * key_cols, :].astype(bf)

    def ring_a(r):
        return remote(kx.at[r], kx.at[r], a_send.at[r], kx_recv.at[r], "sp", y_a)

    def ring_b(r):
        return remote(kx.at[r], kx.at[r], b_send.at[r], kx_recv.at[r], "sp", y_b)

    def needs(row, at):
        low = jnp.where(at >= deep, at - deep + 1, 0)
        high = jnp.where(at >= deep, at, jnp.maximum(at, deep - 1 - at))
        return (row >= low) & (row <= high)

    def column(d):
        target = lax.rem(z + d, nz)
        return target, remote(
            kx.at[far], kx.at[far], z_send.at[d - 1], kx_recv.at[far],
            "sp", (target * ny + y) * 2 + side,
        )

    ring_a(far).start()
    if b_hops:
        ring_b(far).start()
    for d in range(1, nz):
        target, copy = column(d)

        @pl.when(needs(z, target))
        def _():
            copy.start()

    scale = HEAD ** -0.5
    for h in range(heads):
        qa[side, 0:key_cols, h * local_rows:(h + 1) * local_rows] = (
            proj[h * HEAD:(h + 1) * HEAD, :].astype(bf) * bf(scale)
        )

    q_half = pl.ds(0, key_cols)
    q_copy = remote(qa.at[side, q_half], qa.at[side, q_half], q_send, q_recv, "sp", mate)
    q_copy.start()
    partner_q = remote(qa.at[side, q_half], qa.at[2 + side, q_half], pq_send, pq_recv, "sp", partner)
    forward_q = remote(qa.at[2 + side, q_half], qa.at[2 + side, q_half], fq_send, fq_recv, "sp", mate)

    @pl.when(heavy)
    def _():
        partner_q.start()

    sum_copy.wait_recv()
    start_rep = jnp.where(side == 1, pair_sum[...], 0.0)
    both = own_sum[...] + pair_sum[...]
    pick = (
        lax.broadcasted_iota(jnp.int32, (8, LANES), 0)
        == lax.div(lax.broadcasted_iota(jnp.int32, (8, LANES), 1), LANES // heads)
    )
    sums[far] = jnp.concatenate(
        [
            jnp.sum(jnp.where(pick, both, 0.0), axis=0, keepdims=True),
            jnp.sum(jnp.where(pick, start_rep, 0.0), axis=0, keepdims=True),
        ],
        axis=1,
    )

    def tell(d):
        return remote(
            sums.at[far], sums.at[far], tot_send.at[d], tot_recv.at[far],
            "sp", lax.rem(far + d, far_n) * 2 + side,
        )

    def hear(d):
        r = lax.rem(far + d, far_n)
        return remote(sums.at[r], sums.at[r], tot_send.at[d], tot_recv.at[r], "sp", r * 2 + side)

    def send_total(d, carry):
        tell(d).start()
        return carry

    lax.fori_loop(1, far_n, send_total, 0)

    for load in loads[5:]:
        load.wait()

    def wo_a(d):
        ref = wo_all.at[lax.rem(x - sign * d + tp, tp), side]
        return remote(ref, ref, wa_send.at[d], wa_recv.at[d], "tp", x_a)

    def wo_b(d):
        ref = wo_all.at[lax.rem(x + sign * d + tp, tp), side]
        return remote(ref, ref, wb_send.at[d], wb_recv.at[d], "tp", x_b)

    def wo_mate(d):
        ref = wo_all.at[lax.rem(x + d, tp), side]
        return remote(ref, ref, wm_send.at[d - 1], wm_recv.at[d - 1], "sp", mate)

    wo_a(0).start()
    if xb_hops:
        wo_b(0).start()

    def doubled(row, h):
        part = row[:, h * LANES:(h + 1) * LANES]
        return jnp.concatenate([part] * (local_rows // LANES), axis=1)

    q_copy.wait_recv()
    key_at = lax.broadcasted_iota(jnp.int32, (local_rows, local_rows), 0) + side * local_rows
    query_at = lax.broadcasted_iota(jnp.int32, (local_rows, local_rows), 1)
    ka = kx[far, 0:ka_rows, :].T
    va = kx[far, key_cols:, :]
    for g in range(2):
        allowed = key_at <= query_at + g * local_rows
        for h in range(heads):
            here = slice(h * local_rows, (h + 1) * local_rows)
            s = jnp.dot(ka, qa[g, :, here], preferred_element_type=f32)
            shift = jnp.concatenate([start_rep[h:h + 1]] * (local_rows // LANES), axis=1)
            s = jnp.where(allowed, s - shift, masked_value)
            top = jnp.max(s, axis=0, keepdims=True)
            peak[g, :, here] = top
            acc[g, :, here] = jnp.dot(va, jnp.exp(s - top).astype(bf), preferred_element_type=f32)
    peak[2:4] = jnp.full((2, 1, lanes), masked_value, f32)
    acc[2:4] = jnp.zeros((2,) + acc.shape[1:], f32)
    weight[1] = jnp.zeros(weight.shape[1:], bf)
    scaling[1] = jnp.ones(scaling.shape[1:], f32)

    def hear_total(d, carry):
        hear(d).wait_recv()
        return carry

    lax.fori_loop(1, far_n, hear_total, 0)
    lower = (
        lax.broadcasted_iota(jnp.int32, (far_n, far_n), 1)
        < lax.broadcasted_iota(jnp.int32, (far_n, far_n), 0)
    )
    below = jnp.where(lower, 1.0, 0.0).astype(bf)
    table = sums[...].reshape(far_n, 2 * LANES)
    t0, t1, t2 = pieces_of(table[:, :LANES])
    before = jnp.dot(below, t2, preferred_element_type=f32)
    before = before + jnp.dot(below, t1, preferred_element_type=f32)
    before = before + jnp.dot(below, t0, preferred_element_type=f32)
    starts = before + table[:, LANES:]
    for h in range(heads):
        at = h * (LANES // heads)
        span = slice(h * LANES, (h + 1) * LANES)
        gq[:, span] = jnp.broadcast_to(before[:, at:at + 1], (far_n, LANES))
        gk[:, span] = jnp.broadcast_to(starts[:, at:at + 1], (far_n, LANES))

    per = jnp.where(heavy, deep, deep + 1)
    items = per * ny

    def item(n):
        step, j = lax.div(n, per), lax.rem(n, per)
        mine = j <= z
        row = jnp.where(mine, z - j, j - z - 1)
        d = lax.div(step + 1, 2)
        odd = lax.rem(step, 2)
        source = lax.rem(y + jnp.where(odd == 1, -d, d) * sign + ny, ny)
        r = row * ny + source
        skip = mine & (row == z) & (source >= y)
        first = mine | (row > z)
        along_a = ((step == 0) | (odd == 1)) & (d < a_hops)
        along_b = (odd == 0) & (d < b_hops)
        return r, jnp.where(mine, 0, 1), skip, first, along_a, along_b

    def arrive(n):
        r, _, _, first, along_a, along_b = item(n)

        @pl.when(first & (r != far))
        def _():
            ring_a(r).wait_recv()

            @pl.when(along_a)
            def _():
                ring_a(r).start()

            @pl.when(along_b)
            def _():
                ring_b(r).start()

        if nz > 1:
            light = jnp.logical_not(heavy)

            @pl.when(light & (n == 0))
            def _():
                partner_q.wait_recv()
                forward_q.start()

            @pl.when(light & (n == z + 1))
            def _():
                forward_q.wait_recv()

    def score_stage(n, b):
        r, q, _, _, _, _ = item(n)
        ka = kx[r, 0:ka_rows, :].T

        def run(g, here):
            s = jnp.dot(ka, qa[2 * q + g, :, here], preferred_element_type=f32)
            score[b, g, :, here] = s
            tile_max[b, g, :, here] = jnp.max(s, axis=0, keepdims=True)

        return run

    def weight_stage(n, b):
        r, q, skip, _, _, _ = item(n)
        chip = jnp.where(q == 0, far, partner_far)
        offset = gq[pl.ds(chip, 1), :] - gk[pl.ds(r, 1), :]
        offset = jnp.where(skip, skipped_value, offset)

        def run(g, here, h):
            o = doubled(offset, h)
            old = peak[2 * q + g, :, here]
            new = jnp.maximum(old, tile_max[b, g, :, here] + o)
            weight[b, g, :, here] = jnp.exp(score[b, g, :, here] - (new - o)).astype(bf)
            scaling[b, g, :, here] = jnp.exp(old - new)
            peak[2 * q + g, :, here] = new

        return run

    def sum_stage(n, b):
        r, q, _, _, _, _ = item(n)
        va = kx[r, key_cols:, :]

        def run(g, here):
            term = jnp.dot(va, weight[b, g, :, here], preferred_element_type=f32)
            acc[2 * q + g, :, here] = acc[2 * q + g, :, here] * scaling[b, g, :, here] + term

        return run

    tiles = [(g, h, slice(h * local_rows, (h + 1) * local_rows)) for g in range(2) for h in range(heads)]
    arrive(jnp.int32(0))
    begin = score_stage(jnp.int32(0), 0)
    for g, h, here in tiles:
        begin(g, here)

    def trip(i, carry):
        n = 2 * i

        @pl.when(n + 1 < items)
        def _():
            arrive(n + 1)

        @pl.when(n + 2 < items)
        def _():
            arrive(n + 2)

        @pl.when(i == lax.div(items, 4))
        def _():
            wo_a(0).wait_recv()
            if xa_hops > 1:
                wo_a(1).start()
            if xb_hops:
                wo_b(0).wait_recv()

        @pl.when(i == lax.div(items * 7, 16))
        def _():
            if xa_hops > 1:
                wo_a(1).wait_recv()
            for d in range(1, tp):
                wo_mate(d).start()

        for b in range(2):
            now = n + b
            scores = score_stage(jnp.minimum(now + 1, items - 1), 1 - b)
            weights = weight_stage(now, b)
            terms = sum_stage(jnp.maximum(now - 1, 0), 1 - b)
            for g, h, here in tiles:
                scores(g, here)
                weights(g, here, h)
                terms(g, here)
        return carry

    lax.fori_loop(0, lax.div(items, 2), trip, 0)
    finish = sum_stage(items - 1, 1)
    for g, h, here in tiles:
        finish(g, here)

    mass_at, peak_at = 3 * heads, 3 * heads + 1
    cut = 8

    def to_mate(q):
        return remote(
            acc.at[2 * q + 1 - side, pl.ds(cut, ka_rows - cut)], x_in.at[q],
            x_send.at[q], x_recv.at[q], "sp", mate,
        )

    def merged(q):
        mine = 2 * q + side
        a_mass, a_peak = acc[mine, mass_at:mass_at + 1, :], peak[mine]
        b_mass, b_peak = x_in[q, mass_at - cut:mass_at - cut + 1, :], x_in[q, peak_at - cut:peak_at - cut + 1, :]
        top = jnp.maximum(a_peak, b_peak)
        wa, wb = jnp.exp(a_peak - top), jnp.exp(b_peak - top)
        return top, a_mass * wa + b_mass * wb, wa, wb

    def sums_of(q, wa, wb, here):
        return (
            acc[2 * q + side, AUG:, here] * wa[:, here] + x_in[q, AUG - cut:, here] * wb[:, here]
        )

    for q in range(2):
        acc[2 * q + 1 - side, peak_at:peak_at + 1, :] = peak[2 * q + 1 - side]
    ret_copies = [
        remote(ret_o, in_o, r_send.at[0], r_recv.at[0], "sp", partner),
        remote(ret_s, in_s, r_send.at[1], r_recv.at[1], "sp", partner),
    ]

    @pl.when(jnp.logical_not(heavy))
    def _():
        to_mate(1).start()
        to_mate(0).start()
        to_mate(1).wait_recv()
        top, mass, wa, wb = merged(1)
        inverse = 1.0 / mass
        for h in range(heads):
            here = slice(h * local_rows, (h + 1) * local_rows)
            ret_o[:, here] = (sums_of(1, wa, wb, here) * inverse[:, here]).astype(bf)
        ret_s[0:1, :] = top
        ret_s[1:2, :] = mass
        for copy in ret_copies:
            copy.start()
        to_mate(0).wait_recv()
        top, mass, wa, wb = merged(0)
        inverse = 1.0 / mass
        for h in range(heads):
            here = slice(h * local_rows, (h + 1) * local_rows)
            att_t[h * HEAD:(h + 1) * HEAD, :] = (sums_of(0, wa, wb, here) * inverse[:, here]).astype(bf)

    @pl.when(heavy)
    def _():
        to_mate(0).start()
        to_mate(0).wait_recv()
        top, mass, wa, wb = merged(0)
        for copy in ret_copies:
            copy.wait_recv()
        r_top, r_mass = in_s[0:1, :], in_s[1:2, :]
        best = jnp.maximum(top, r_top)
        w_own, w_far = jnp.exp(top - best), jnp.exp(r_top - best) * r_mass
        inverse = 1.0 / (mass * w_own + w_far)
        w_own, w_far = w_own * inverse, w_far * inverse
        for h in range(heads):
            here = slice(h * local_rows, (h + 1) * local_rows)
            att_t[h * HEAD:(h + 1) * HEAD, :] = (
                sums_of(0, wa, wb, here) * w_own[:, here] + in_o[:, here].astype(f32) * w_far[:, here]
            ).astype(bf)

    att_out[...] = att_t[...].T.reshape(tp, rows, q_cols)

    def att_copy(d):
        to = lax.rem(x + d, tp)
        return remote(att_out.at[to], att_all.at[x], att_send.at[d - 1], att_recv.at[d - 1], "tp", to)

    for d in range(1, tp):
        att_copy(d).start()
    att_all[x] = att_out[x]
    for d in range(1, tp):
        wo_mate(d).wait_recv()
    for d in range(1, tp):
        att_copy(d).wait_recv()
    for k in range(4):
        span = slice(k * (out_cols // 4), (k + 1) * (out_cols // 4))
        value = None
        for r in range(tp):
            term = jnp.dot(
                att_all[r], wo_all[r, :, :, span].reshape(q_cols, out_cols // 4),
                preferred_element_type=f32,
            ).astype(bf).astype(f32)
            value = term if value is None else value + term
        out[:, span] = value.astype(bf)

    for k in range(chunks):
        for d in range(xa_hops):
            tok_a(d, k).wait_send()
        for d in range(xb_hops):
            tok_b(d, k).wait_send()
    sum_copy.wait_send()
    q_copy.wait_send()

    def drain_total(d, carry):
        tell(d).wait_send()
        return carry

    lax.fori_loop(1, far_n, drain_total, 0)
    for d in range(xa_hops):
        wo_a(d).wait_send()
    for d in range(xb_hops):
        wo_b(d).wait_send()
    for d in range(1, tp):
        wo_mate(d).wait_send()
        att_copy(d).wait_send()
    for d in range(1, nz):
        target, copy = column(d)

        @pl.when(needs(z, target))
        def _():
            copy.wait_send()

    def drain(n, carry):
        r, _, _, first, along_a, along_b = item(n)

        @pl.when(first & along_a)
        def _():
            ring_a(r).wait_send()

        @pl.when(first & along_b)
        def _():
            ring_b(r).wait_send()

        return carry

    lax.fori_loop(0, items, drain, 0)
    to_mate(0).wait_send()

    @pl.when(heavy)
    def _():
        partner_q.wait_send()

    @pl.when(jnp.logical_not(heavy))
    def _():
        forward_q.wait_send()
        to_mate(1).wait_send()
        for copy in ret_copies:
            copy.wait_send()


def shards(ny, tokens, w_query, w_key, w_value, w_gate, gate_bias, w_output):
    sp = lax.axis_size("sp")
    tp = lax.axis_size("tp")
    rows, width = tokens.shape
    local_rows = rows * tp
    q_cols, key_cols, heads = w_query.shape[1], w_key.shape[1], w_gate.shape[1]
    out_cols = w_output.shape[1]
    assert key_cols == HEAD and heads == 4 and q_cols == heads * HEAD
    chunks = 4 if width % 512 == 0 else 2
    far_n = sp // 2
    nz = far_n // ny
    lanes = heads * local_rows
    ka_rows = key_cols + AUG
    xa, xb = tp // 2, max(tp // 2 - 1, 1)
    dma = pltpu.SemaphoreType.DMA
    hbm_spec = pl.BlockSpec(memory_space=pltpu.HBM)
    vmem_spec = pl.BlockSpec(memory_space=pltpu.VMEM)
    operands = (tokens, w_query, w_key.T, w_value.T, w_gate.T, gate_bias, w_output)
    vmem = pltpu.VMEM
    return pl.pallas_call(
        functools.partial(kernel, sp, tp, ny, chunks),
        out_shape=jax.ShapeDtypeStruct((rows, out_cols), bf),
        in_specs=[hbm_spec] * 7,
        out_specs=vmem_spec,
        scratch_shapes=[
            vmem((tp, rows, width), bf),
            vmem((width, q_cols), bf),
            vmem((q_cols + 2 * key_cols + AUG, width), bf),
            vmem((heads, width), bf),
            vmem((tp, 2, q_cols // 2, out_cols), bf),
            vmem((q_cols + 2 * key_cols + AUG, local_rows), f32),
            vmem((far_n, ka_rows + key_cols, local_rows), bf),
            vmem((4, ka_rows, lanes), bf),
            vmem((8, LANES), f32),
            vmem((8, LANES), f32),
            vmem((far_n, 1, 2 * LANES), f32),
            vmem((far_n, heads * LANES), f32),
            vmem((far_n, heads * LANES), f32),
            vmem((2, 2, local_rows, lanes), f32),
            vmem((2, 2, local_rows, lanes), bf),
            vmem((2, 2, 1, lanes), f32),
            vmem((2, 2, 1, lanes), f32),
            vmem((4, 1, lanes), f32),
            vmem((4, ka_rows, lanes), f32),
            vmem((2, ka_rows - 8, lanes), f32),
            vmem((key_cols, lanes), bf),
            vmem((8, lanes), f32),
            vmem((key_cols, lanes), bf),
            vmem((8, lanes), f32),
            vmem((q_cols, local_rows), bf),
            vmem((tp, rows, q_cols), bf),
            vmem((tp, rows, q_cols), bf),
            pltpu.SMEM((heads,), f32),
            dma((7,)),
            dma,
            dma((xa, chunks)),
            dma((xa, chunks)),
            dma((xb, chunks)),
            dma((xb, chunks)),
            dma,
            dma,
            dma((far_n,)),
            dma((far_n,)),
            dma,
            dma,
            dma,
            dma,
            dma,
            dma,
            dma((nz,)),
            dma((far_n,)),
            dma((far_n,)),
            dma((far_n,)),
            dma((xa,)),
            dma((xa,)),
            dma((xb,)),
            dma((xb,)),
            dma((tp - 1,)),
            dma((tp - 1,)),
            dma((2,)),
            dma((2,)),
            dma((2,)),
            dma((2,)),
            dma((tp - 1,)),
            dma((tp - 1,)),
        ],
        compiler_params=pltpu.CompilerParams(
            collective_id=0, has_side_effects=True, vmem_limit_bytes=60 << 20
        ),
    )(*(pltpu.with_memory_space_constraint(x, pltpu.HBM) for x in operands))


def solution(mesh):
    return jax.shard_map(
        functools.partial(shards, min(RING, mesh.shape["sp"] // 4)),
        mesh=mesh,
        in_specs=(
            P(("sp", "tp"), None),
            P(None, "tp"),
            P(None, "tp"),
            P(None, "tp"),
            P(None, "tp"),
            P("tp"),
            P("tp", None),
        ),
        out_specs=P(("sp", "tp"), None),
        check_vma=False,
    )
```

time: 296 us -> 96.9 us (0.33)
  the two profiles are of different devices: /device:TPU:505 before, /device:TPU:1 now
where the time goes in v1:
time: 96.9 us; the launch traced here: 96.7 us
  Pallas kernels  95.1 us (98%)
  local copies, waits for them, and re-layouts  1.67 us (2%)
    pallas_call x1, Pallas kernels, shards(): pl.pallas_call(functools.partial(kernel, sp, tp, ny, chunks), out_shape=j...  95.1 us

profile of v1, /device:TPU:1, one launch (start us, length us, event | category | flops | bytes accessed | tf_op | source)
XLA Modules:
  0.0 96.7 jit_solution(1549048028902801468)
XLA Ops:
  0.0 95.1 %shard_map.73 = bf16[64,2048]{1,0:T(8,128)(2,1)} custom-call(bf16[64,2048]{1,0:T(8,128)(2,1)} %tokens.1, bf16[2048,256]{1,0:T(8,128)(2,1)} %w_query.1, bf16[64,2048]{1,0:T(8,128)(2,1)} %bitcast.3, bf16[64,2048]{1,0:T(8,128)(2,1)} %bitcast.4, bf16[4,2048]{1,0:T(4,128)(2,1)} %bitcast.5, f32[4]{0:T(128)} %bias_in.1, bf16[256,2048]{1,0:T(8,128)(2,1)} %w_output.1), custom_call_target="tpu_custom_call" | custom-call | tf_op jit(solution)/shard_map/pallas_call | solution.py:616
  95.1 1.7 %copy.9 = bf16[64,2048]{1,0:T(8,128)(2,1)} copy(bf16[64,2048]{1,0:T(8,128)(2,1)} %shard_map.73) | data formatting | bytes 524288

commit v2 on v1

--- a/solution.py
+++ b/solution.py
@@ -11,6 +11,8 @@
 LANES = 128
 AUG = 16
 RING = 8
+CUT = 8
+MASS, PEAK = 12 - CUT, 13 - CUT
 masked_value = -1e30
 skipped_value = -1e38
 MESH = pl.DeviceIdType.MESH
@@ -29,8 +31,8 @@
     sp, tp, ny, chunks,
     tokens, w_query, w_key, w_value, w_gate, bias_in, w_output,
     out,
-    tok, wq_raw, wt, w_g, wo_all, proj, kx, qa, own_sum, pair_sum, sums, gk, gq,
-    score, weight, tile_max, scaling, peak, acc, x_in, ret_o, ret_s, in_o, in_s,
+    tok, wq_raw, wt, w_g, wo_all, proj, kx, qa, sums, pair_sums, gk, gq,
+    score, tile_max, peak, acc, x_in, ret_o, ret_s, in_o, in_s,
     att_t, att_out, att_all, bias,
     local_sem, own_sem, ta_send, ta_recv, tb_send, tb_recv,
     sum_send, sum_recv, tot_send, tot_recv,
@@ -134,15 +136,20 @@
     for i in range(4):
         qa[i, key_cols:ka_rows, :] = pattern
 
+    def relay(d, k):
+        tok_a(d - 1, k).wait_recv()
+        if d < xa_hops:
+            tok_a(d, k).start()
+        if d <= xb_hops:
+            tok_b(d - 1, k).wait_recv()
+            if d < xb_hops:
+                tok_b(d, k).start()
+
+    for d in range(1, xa_hops):
+        for k in range(chunks):
+            relay(d, k)
     for k in range(chunks):
-        for d in range(1, xa_hops + 1):
-            tok_a(d - 1, k).wait_recv()
-            if d < xa_hops:
-                tok_a(d, k).start()
-            if d <= xb_hops:
-                tok_b(d - 1, k).wait_recv()
-                if d < xb_hops:
-                    tok_b(d, k).start()
+        relay(xa_hops, k)
         here = tok[:, :, k * piece:(k + 1) * piece].reshape(local_rows, piece)
         part = lax.dot_general(
             wt[:, k * piece:(k + 1) * piece], here, (((1,), (1,)), ((), ())),
@@ -168,9 +175,28 @@
     total = jnp.dot(g2, ones, preferred_element_type=f32)
     total = total + jnp.dot(g1, ones, preferred_element_type=f32)
     total = total + jnp.dot(g0, ones, preferred_element_type=f32)
-    own_sum[...] = jnp.broadcast_to(total[:, local_rows - 1:], (8, LANES))
-    sum_copy = remote(own_sum, pair_sum, sum_send, sum_recv, "sp", mate)
-    sum_copy.start()
+    pick = (
+        lax.broadcasted_iota(jnp.int32, (8, LANES), 0)
+        == lax.div(lax.broadcasted_iota(jnp.int32, (8, LANES), 1), LANES // heads)
+    )
+    block_sum = jnp.broadcast_to(total[:, local_rows - 1:], (8, LANES))
+    sums[far] = jnp.sum(jnp.where(pick, block_sum, 0.0), axis=0, keepdims=True)
+
+    def tell(d):
+        return remote(
+            sums.at[far], sums.at[far], tot_send.at[d], tot_recv.at[far],
+            "sp", lax.rem(far + d, far_n) * 2 + side,
+        )
+
+    def hear(d):
+        r = lax.rem(far + d, far_n)
+        return remote(sums.at[r], sums.at[r], tot_send.at[d], tot_recv.at[r], "sp", r * 2 + side)
+
+    def send_total(d, carry):
+        tell(d).start()
+        return carry
+
+    lax.fori_loop(1, far_n, send_total, 0)
 
     s0, s1, s2 = [p.astype(f32)[:heads] for p in pieces_of(-total)]
     last = jnp.where(lax.broadcasted_iota(jnp.int32, (AUG - 3 * heads, local_rows), 0) == 0, 1.0, 0.0)
@@ -221,37 +247,6 @@
     @pl.when(heavy)
     def _():
         partner_q.start()
-
-    sum_copy.wait_recv()
-    start_rep = jnp.where(side == 1, pair_sum[...], 0.0)
-    both = own_sum[...] + pair_sum[...]
-    pick = (
-        lax.broadcasted_iota(jnp.int32, (8, LANES), 0)
-        == lax.div(lax.broadcasted_iota(jnp.int32, (8, LANES), 1), LANES // heads)
-    )
-    sums[far] = jnp.concatenate(
-        [
-            jnp.sum(jnp.where(pick, both, 0.0), axis=0, keepdims=True),
-            jnp.sum(jnp.where(pick, start_rep, 0.0), axis=0, keepdims=True),
-        ],
-        axis=1,
-    )
-
-    def tell(d):
-        return remote(
-            sums.at[far], sums.at[far], tot_send.at[d], tot_recv.at[far],
-            "sp", lax.rem(far + d, far_n) * 2 + side,
-        )
-
-    def hear(d):
-        r = lax.rem(far + d, far_n)
-        return remote(sums.at[r], sums.at[r], tot_send.at[d], tot_recv.at[r], "sp", r * 2 + side)
-
-    def send_total(d, carry):
-        tell(d).start()
-        return carry
-
-    lax.fori_loop(1, far_n, send_total, 0)
 
     for load in loads[5:]:
         load.wait()
@@ -286,84 +281,109 @@
         for h in range(heads):
             here = slice(h * local_rows, (h + 1) * local_rows)
             s = jnp.dot(ka, qa[g, :, here], preferred_element_type=f32)
-            shift = jnp.concatenate([start_rep[h:h + 1]] * (local_rows // LANES), axis=1)
-            s = jnp.where(allowed, s - shift, masked_value)
+            s = jnp.where(allowed, s, masked_value)
             top = jnp.max(s, axis=0, keepdims=True)
             peak[g, :, here] = top
-            acc[g, :, here] = jnp.dot(va, jnp.exp(s - top).astype(bf), preferred_element_type=f32)
+            term = jnp.dot(va, jnp.exp(s - top).astype(bf), preferred_element_type=f32)
+            acc[g, :, here] = term[CUT:]
     peak[2:4] = jnp.full((2, 1, lanes), masked_value, f32)
     acc[2:4] = jnp.zeros((2,) + acc.shape[1:], f32)
-    weight[1] = jnp.zeros(weight.shape[1:], bf)
-    scaling[1] = jnp.ones(scaling.shape[1:], f32)
+
+    top_row = jnp.where(heavy, z, jnp.maximum(z, other_z - deep))
+    row_n = jnp.where(heavy, deep, top_row + 1)
+
+    def event(e):
+        step, at = lax.div(e, row_n), lax.rem(e, row_n)
+        d = lax.div(step + 1, 2)
+        odd = lax.rem(step, 2)
+        source = lax.rem(y + jnp.where(odd == 1, -d, d) * sign + ny, ny)
+        along_a = ((step == 0) | (odd == 1)) & (d < a_hops)
+        along_b = (odd == 0) & (d < b_hops)
+        return (top_row - at) * ny + source, along_a, along_b
+
+    def arrive(e, carry):
+        r, along_a, along_b = event(e)
+
+        @pl.when(r != far)
+        def _():
+            ring_a(r).wait_recv()
+
+            @pl.when(along_a)
+            def _():
+                ring_a(r).start()
+
+            @pl.when(along_b)
+            def _():
+                ring_b(r).start()
+
+        return carry
+
+    lax.fori_loop(0, row_n, arrive, 0)
 
     def hear_total(d, carry):
         hear(d).wait_recv()
         return carry
 
     lax.fori_loop(1, far_n, hear_total, 0)
+    sum_copy = remote(sums, pair_sums, sum_send, sum_recv, "sp", mate)
+    sum_copy.start()
     lower = (
         lax.broadcasted_iota(jnp.int32, (far_n, far_n), 1)
         < lax.broadcasted_iota(jnp.int32, (far_n, far_n), 0)
     )
     below = jnp.where(lower, 1.0, 0.0).astype(bf)
-    table = sums[...].reshape(far_n, 2 * LANES)
-    t0, t1, t2 = pieces_of(table[:, :LANES])
+    sum_copy.wait_recv()
+    pair_table = pair_sums[...].reshape(far_n, LANES)
+    start_table = jnp.where(side == 1, pair_table, 0.0)
+    t0, t1, t2 = pieces_of(sums[...].reshape(far_n, LANES) + pair_table)
     before = jnp.dot(below, t2, preferred_element_type=f32)
     before = before + jnp.dot(below, t1, preferred_element_type=f32)
     before = before + jnp.dot(below, t0, preferred_element_type=f32)
-    starts = before + table[:, LANES:]
+    starts = before + start_table
     for h in range(heads):
         at = h * (LANES // heads)
         span = slice(h * LANES, (h + 1) * LANES)
         gq[:, span] = jnp.broadcast_to(before[:, at:at + 1], (far_n, LANES))
         gk[:, span] = jnp.broadcast_to(starts[:, at:at + 1], (far_n, LANES))
 
-    per = jnp.where(heavy, deep, deep + 1)
+    own_shift = gq[pl.ds(far, 1), :] - gk[pl.ds(far, 1), :]
+    for g in range(2):
+        for h in range(heads):
+            here = slice(h * local_rows, (h + 1) * local_rows)
+            peak[g, :, here] = peak[g, :, here] + doubled(own_shift, h)
+
+    lent = jnp.where(heavy, 0, other_z - deep + 1)
+    kept = jnp.where(heavy, deep, z + 1)
+    lag = jnp.where(heavy, 0, min(2, ny - 1))
+    per = kept + lent
+    head_items = lag * lent
+    core_items = (ny - lag) * per
     items = per * ny
+    partner_items = jnp.where(heavy, items, head_items + core_items - kept)
 
     def item(n):
-        step, j = lax.div(n, per), lax.rem(n, per)
-        mine = j <= z
-        row = jnp.where(mine, z - j, j - z - 1)
+        in_head = n < head_items
+        in_core = n < head_items + core_items
+        m = jnp.where(in_head, n, jnp.where(in_core, n - head_items, n - head_items - core_items))
+        group = jnp.where(in_head, jnp.maximum(lent, 1), jnp.where(in_core, per, kept))
+        t, j = lax.div(m, group), lax.rem(m, group)
+        borrowed = in_head | (in_core & (j < lent))
+        k = jnp.where(borrowed, j, jnp.where(in_core, j - lent, j))
+        arrived = jnp.where(in_head, t, jnp.where(in_core, t + lag, ny))
+        step = jnp.where(borrowed, arrived, jnp.where(in_core, t, t + ny - lag))
+        row = jnp.where(borrowed, other_z - deep - k, z - k)
         d = lax.div(step + 1, 2)
         odd = lax.rem(step, 2)
         source = lax.rem(y + jnp.where(odd == 1, -d, d) * sign + ny, ny)
-        r = row * ny + source
-        skip = mine & (row == z) & (source >= y)
-        first = mine | (row > z)
-        along_a = ((step == 0) | (odd == 1)) & (d < a_hops)
-        along_b = (odd == 0) & (d < b_hops)
-        return r, jnp.where(mine, 0, 1), skip, first, along_a, along_b
-
-    def arrive(n):
-        r, _, _, first, along_a, along_b = item(n)
-
-        @pl.when(first & (r != far))
-        def _():
-            ring_a(r).wait_recv()
-
-            @pl.when(along_a)
-            def _():
-                ring_a(r).start()
-
-            @pl.when(along_b)
-            def _():
-                ring_b(r).start()
-
-        if nz > 1:
-            light = jnp.logical_not(heavy)
-
-            @pl.when(light & (n == 0))
-            def _():
-                partner_q.wait_recv()
-                forward_q.start()
-
-            @pl.when(light & (n == z + 1))
-            def _():
-                forward_q.wait_recv()
+        skip = jnp.logical_not(borrowed) & (row == z) & (source >= y)
+        exact = borrowed | heavy
+        need = jnp.where(
+            exact, arrived * row_n + top_row - row + 1, jnp.minimum(arrived + 1, ny) * row_n
+        )
+        return row * ny + source, jnp.where(borrowed, 1, 0), skip, jnp.maximum(need, row_n)
 
     def score_stage(n, b):
-        r, q, _, _, _, _ = item(n)
+        r, q, _, _ = item(n)
         ka = kx[r, 0:ka_rows, :].T
 
         def run(g, here):
@@ -373,8 +393,9 @@
 
         return run
 
-    def weight_stage(n, b):
-        r, q, skip, _, _, _ = item(n)
+    def sum_stage(n, b):
+        r, q, skip, _ = item(n)
+        va = kx[r, key_cols:, :]
         chip = jnp.where(q == 0, far, partner_far)
         offset = gq[pl.ds(chip, 1), :] - gk[pl.ds(r, 1), :]
         offset = jnp.where(skip, skipped_value, offset)
@@ -383,38 +404,30 @@
             o = doubled(offset, h)
             old = peak[2 * q + g, :, here]
             new = jnp.maximum(old, tile_max[b, g, :, here] + o)
-            weight[b, g, :, here] = jnp.exp(score[b, g, :, here] - (new - o)).astype(bf)
-            scaling[b, g, :, here] = jnp.exp(old - new)
+            weight = jnp.exp(score[b, g, :, here] - (new - o)).astype(bf)
+            rescale = jnp.exp(old - new)
             peak[2 * q + g, :, here] = new
+            term = jnp.dot(va, weight, preferred_element_type=f32)
+            acc[2 * q + g, :, here] = acc[2 * q + g, :, here] * rescale + term[CUT:]
 
         return run
 
-    def sum_stage(n, b):
-        r, q, _, _, _, _ = item(n)
-        va = kx[r, key_cols:, :]
-
-        def run(g, here):
-            term = jnp.dot(va, weight[b, g, :, here], preferred_element_type=f32)
-            acc[2 * q + g, :, here] = acc[2 * q + g, :, here] * scaling[b, g, :, here] + term
-
-        return run
-
     tiles = [(g, h, slice(h * local_rows, (h + 1) * local_rows)) for g in range(2) for h in range(heads)]
-    arrive(jnp.int32(0))
+
+    @pl.when(jnp.logical_not(heavy))
+    def _():
+        partner_q.wait_recv()
+        forward_q.start()
+        forward_q.wait_recv()
+
+    lax.fori_loop(row_n, item(jnp.int32(0))[3], arrive, 0)
     begin = score_stage(jnp.int32(0), 0)
     for g, h, here in tiles:
         begin(g, here)
 
     def trip(i, carry):
         n = 2 * i
-
-        @pl.when(n + 1 < items)
-        def _():
-            arrive(n + 1)
-
-        @pl.when(n + 2 < items)
-        def _():
-            arrive(n + 2)
+        lax.fori_loop(item(n)[3], item(jnp.minimum(n + 2, items - 1))[3], arrive, 0)
 
         @pl.when(i == lax.div(items, 4))
         def _():
@@ -434,52 +447,41 @@
         for b in range(2):
             now = n + b
             scores = score_stage(jnp.minimum(now + 1, items - 1), 1 - b)
-            weights = weight_stage(now, b)
-            terms = sum_stage(jnp.maximum(now - 1, 0), 1 - b)
+            sums_now = sum_stage(now, b)
             for g, h, here in tiles:
                 scores(g, here)
-                weights(g, here, h)
-                terms(g, here)
+                sums_now(g, here, h)
         return carry
-
-    lax.fori_loop(0, lax.div(items, 2), trip, 0)
-    finish = sum_stage(items - 1, 1)
-    for g, h, here in tiles:
-        finish(g, here)
-
-    mass_at, peak_at = 3 * heads, 3 * heads + 1
-    cut = 8
 
     def to_mate(q):
         return remote(
-            acc.at[2 * q + 1 - side, pl.ds(cut, ka_rows - cut)], x_in.at[q],
-            x_send.at[q], x_recv.at[q], "sp", mate,
+            acc.at[2 * q + 1 - side], x_in.at[q], x_send.at[q], x_recv.at[q], "sp", mate
         )
 
     def merged(q):
         mine = 2 * q + side
-        a_mass, a_peak = acc[mine, mass_at:mass_at + 1, :], peak[mine]
-        b_mass, b_peak = x_in[q, mass_at - cut:mass_at - cut + 1, :], x_in[q, peak_at - cut:peak_at - cut + 1, :]
+        a_mass, a_peak = acc[mine, MASS:MASS + 1, :], peak[mine]
+        b_mass, b_peak = x_in[q, MASS:MASS + 1, :], x_in[q, PEAK:PEAK + 1, :]
         top = jnp.maximum(a_peak, b_peak)
         wa, wb = jnp.exp(a_peak - top), jnp.exp(b_peak - top)
         return top, a_mass * wa + b_mass * wb, wa, wb
 
     def sums_of(q, wa, wb, here):
         return (
-            acc[2 * q + side, AUG:, here] * wa[:, here] + x_in[q, AUG - cut:, here] * wb[:, here]
+            acc[2 * q + side, AUG - CUT:, here] * wa[:, here] + x_in[q, AUG - CUT:, here] * wb[:, here]
         )
 
-    for q in range(2):
-        acc[2 * q + 1 - side, peak_at:peak_at + 1, :] = peak[2 * q + 1 - side]
     ret_copies = [
         remote(ret_o, in_o, r_send.at[0], r_recv.at[0], "sp", partner),
         remote(ret_s, in_s, r_send.at[1], r_recv.at[1], "sp", partner),
     ]
+    half_trips = lax.div(partner_items + 1, 2)
+    lax.fori_loop(0, half_trips, trip, 0)
 
     @pl.when(jnp.logical_not(heavy))
     def _():
+        acc[3 - side, PEAK:PEAK + 1, :] = peak[3 - side]
         to_mate(1).start()
-        to_mate(0).start()
         to_mate(1).wait_recv()
         top, mass, wa, wb = merged(1)
         inverse = 1.0 / mass
@@ -490,8 +492,15 @@
         ret_s[1:2, :] = mass
         for copy in ret_copies:
             copy.start()
-        to_mate(0).wait_recv()
-        top, mass, wa, wb = merged(0)
+
+    lax.fori_loop(half_trips, lax.div(items, 2), trip, 0)
+    acc[1 - side, PEAK:PEAK + 1, :] = peak[1 - side]
+    to_mate(0).start()
+    to_mate(0).wait_recv()
+    top, mass, wa, wb = merged(0)
+
+    @pl.when(jnp.logical_not(heavy))
+    def _():
         inverse = 1.0 / mass
         for h in range(heads):
             here = slice(h * local_rows, (h + 1) * local_rows)
@@ -499,9 +508,6 @@
 
     @pl.when(heavy)
     def _():
-        to_mate(0).start()
-        to_mate(0).wait_recv()
-        top, mass, wa, wb = merged(0)
         for copy in ret_copies:
             copy.wait_recv()
         r_top, r_mass = in_s[0:1, :], in_s[1:2, :]
@@ -524,6 +530,55 @@
     for d in range(1, tp):
         att_copy(d).start()
     att_all[x] = att_out[x]
+    for k in range(chunks):
+        for d in range(xa_hops):
+            tok_a(d, k).wait_send()
+        for d in range(xb_hops):
+            tok_b(d, k).wait_send()
+    sum_copy.wait_send()
+    q_copy.wait_send()
+
+    def drain_total(d, carry):
+        tell(d).wait_send()
+        return carry
+
+    lax.fori_loop(1, far_n, drain_total, 0)
+    for d in range(xa_hops):
+        wo_a(d).wait_send()
+    for d in range(xb_hops):
+        wo_b(d).wait_send()
+    for d in range(1, nz):
+        target, copy = column(d)
+
+        @pl.when(needs(z, target))
+        def _():
+            copy.wait_send()
+
+    def drain(e, carry):
+        r, along_a, along_b = event(e)
+
+        @pl.when(along_a)
+        def _():
+            ring_a(r).wait_send()
+
+        @pl.when(along_b)
+        def _():
+            ring_b(r).wait_send()
+
+        return carry
+
+    lax.fori_loop(0, row_n * ny, drain, 0)
+    to_mate(0).wait_send()
+
+    @pl.when(heavy)
+    def _():
+        partner_q.wait_send()
+
+    @pl.when(jnp.logical_not(heavy))
+    def _():
+        forward_q.wait_send()
+        to_mate(1).wait_send()
+
     for d in range(1, tp):
         wo_mate(d).wait_recv()
     for d in range(1, tp):
@@ -539,57 +594,12 @@
             value = term if value is None else value + term
         out[:, span] = value.astype(bf)
 
-    for k in range(chunks):
-        for d in range(xa_hops):
-            tok_a(d, k).wait_send()
-        for d in range(xb_hops):
-            tok_b(d, k).wait_send()
-    sum_copy.wait_send()
-    q_copy.wait_send()
-
-    def drain_total(d, carry):
-        tell(d).wait_send()
-        return carry
-
-    lax.fori_loop(1, far_n, drain_total, 0)
-    for d in range(xa_hops):
-        wo_a(d).wait_send()
-    for d in range(xb_hops):
-        wo_b(d).wait_send()
     for d in range(1, tp):
         wo_mate(d).wait_send()
         att_copy(d).wait_send()
-    for d in range(1, nz):
-        target, copy = column(d)
-
-        @pl.when(needs(z, target))
-        def _():
-            copy.wait_send()
-
-    def drain(n, carry):
-        r, _, _, first, along_a, along_b = item(n)
-
-        @pl.when(first & along_a)
-        def _():
-            ring_a(r).wait_send()
-
-        @pl.when(first & along_b)
-        def _():
-            ring_b(r).wait_send()
-
-        return carry
-
-    lax.fori_loop(0, items, drain, 0)
-    to_mate(0).wait_send()
-
-    @pl.when(heavy)
-    def _():
-        partner_q.wait_send()
 
     @pl.when(jnp.logical_not(heavy))
     def _():
-        forward_q.wait_send()
-        to_mate(1).wait_send()
         for copy in ret_copies:
             copy.wait_send()
 
@@ -602,7 +612,7 @@
     q_cols, key_cols, heads = w_query.shape[1], w_key.shape[1], w_gate.shape[1]
     out_cols = w_output.shape[1]
     assert key_cols == HEAD and heads == 4 and q_cols == heads * HEAD
-    chunks = 4 if width % 512 == 0 else 2
+    chunks = 8 if width % 1024 == 0 else 2
     far_n = sp // 2
     nz = far_n // ny
     lanes = heads * local_rows
@@ -627,18 +637,15 @@
             vmem((q_cols + 2 * key_cols + AUG, local_rows), f32),
             vmem((far_n, ka_rows + key_cols, local_rows), bf),
             vmem((4, ka_rows, lanes), bf),
-            vmem((8, LANES), f32),
-            vmem((8, LANES), f32),
-            vmem((far_n, 1, 2 * LANES), f32),
+            vmem((far_n, 1, LANES), f32),
+            vmem((far_n, 1, LANES), f32),
             vmem((far_n, heads * LANES), f32),
             vmem((far_n, heads * LANES), f32),
             vmem((2, 2, local_rows, lanes), f32),
-            vmem((2, 2, local_rows, lanes), bf),
-            vmem((2, 2, 1, lanes), f32),
             vmem((2, 2, 1, lanes), f32),
             vmem((4, 1, lanes), f32),
-            vmem((4, ka_rows, lanes), f32),
-            vmem((2, ka_rows - 8, lanes), f32),
+            vmem((4, ka_rows - CUT, lanes), f32),
+            vmem((2, ka_rows - CUT, lanes), f32),
             vmem((key_cols, lanes), bf),
             vmem((8, lanes), f32),
             vmem((key_cols, lanes), bf),

time: 96.9 us -> 81.7 us (0.84)
  the two profiles are of different devices: /device:TPU:1 before, /device:TPU:192 now
where the time goes in v2:
time: 81.7 us; the launch traced here: 81.6 us
  Pallas kernels  79.9 us (98%)
  local copies, waits for them, and re-layouts  1.67 us (2%)
    pallas_call x1, Pallas kernels, shards(): pl.pallas_call(functools.partial(kernel, sp, tp, ny, chunks), out_shape=j...  79.9 us
    unnamed x1, local copies, waits for them, and re-layouts  1.67 us

profile of v2, /device:TPU:192, one launch (start us, length us, event | category | flops | bytes accessed | tf_op | source)
XLA Modules:
  0.0 81.6 jit_solution(218692538807789796)
XLA Ops:
  0.0 79.9 %shard_map.73 = bf16[64,2048]{1,0:T(8,128)(2,1)} custom-call(bf16[64,2048]{1,0:T(8,128)(2,1)} %tokens.1, bf16[2048,256]{1,0:T(8,128)(2,1)} %w_query.1, bf16[64,2048]{1,0:T(8,128)(2,1)} %bitcast.3, bf16[64,2048]{1,0:T(8,128)(2,1)} %bitcast.4, bf16[4,2048]{1,0:T(4,128)(2,1)} %bitcast.5, f32[4]{0:T(128)} %bias_in.1, bf16[256,2048]{1,0:T(8,128)(2,1)} %w_output.1), custom_call_target="tpu_custom_call" | custom-call | tf_op jit(solution)/shard_map/pallas_call | solution.py:626
  79.9 1.7 %copy.9 = bf16[64,2048]{1,0:T(8,128)(2,1)} copy(bf16[64,2048]{1,0:T(8,128)(2,1)} %shard_map.73) | data formatting | bytes 524288

commit v3 on v2

--- a/solution.py
+++ b/solution.py
@@ -27,6 +27,65 @@
     return a, b, c
 
 
+LAG = 6
+
+
+def plan(z, nz, ny):
+    deep = nz // 2
+    heavy = z >= deep
+    kept = range(z - deep + 1, z + 1) if heavy else range(z + 1)
+    lent = () if heavy else range(deep - z)
+    others = sorted(set(kept) | set(lent), key=lambda row: (abs(row - z), row))[1:]
+    own = [(z, step) for step in range(1, ny)]
+    events = []
+    queue = list(own[:-1]) if ny > 2 else list(own)
+    for row in others:
+        events += queue[:2] + [(row, 0)]
+        queue = queue[2:]
+    events += queue
+    late = own[len(own) - 1:] if ny > 2 else []
+    split = [(z - deep if heavy else deep - 1 - z, step) for step in range(min(3, ny - 1))]
+    split = split if deep >= 3 else []
+    shared = split if heavy else []
+    for step in range(1, ny):
+        events += [(row, step) for row in others]
+        if step == 2:
+            events += late
+        if step == 1:
+            events += shared[:1]
+        if step == min(3, ny - 1):
+            events += shared[1:]
+    ahead = min(6, len(events))
+    place = {event: at + 1 for at, event in enumerate(events)}
+    place[(z, 0)] = 0
+    first = [(event, 0) for event in own[:-1]]
+    keep = [event for event in events if event[0] in kept and (event, 0) not in first]
+    lend = ([(z, 0)] if z in lent else []) + [event for event in events if event[0] in lent]
+    lend = [event for event in lend if event not in split]
+    if heavy:
+        items = [(event, 0) for event in events]
+        fast = first[:4]
+        items = fast + [item for item in items if item not in fast]
+    else:
+        items = first[:4]
+        keep = sorted([event for event, _ in first[4:]] + keep, key=lambda event: place[event])
+        waiting = list(keep)
+        for at in range(len(events) + 1):
+            items += [(event, 1) for event in lend if place[event] == at]
+            while waiting and place[waiting[0]] <= at - LAG:
+                items.append((waiting.pop(0), 0))
+        items += [(event, 0) for event in waiting]
+    lent_end = max([at + 1 for at, item in enumerate(items) if item[1] == 1], default=len(items))
+    table, need = [], ahead
+    for (row, step), q in items:
+        need = max(need, place[(row, step)])
+        table.append((row, step, q, 0, need))
+    if len(table) % 2:
+        table.append(table[-1][:2] + (0, 1, need))
+    lent_end = len(table) if heavy else min((lent_end + 1) // 2 * 2, len(table))
+    return events, ahead, table, lent_end
+
+
 def kernel(
     sp, tp, ny, chunks,
     tokens, w_query, w_key, w_value, w_gate, bias_in, w_output,
@@ -35,7 +94,7 @@
     score, tile_max, peak, acc, x_in, ret_o, ret_s, in_o, in_s,
     att_t, att_out, att_all, bias,
     local_sem, own_sem, ta_send, ta_recv, tb_send, tb_recv,
-    sum_send, sum_recv, tot_send, tot_recv,
+    sum_send, sum_recv, tot_send, tot_recv, onward_send,
     q_send, q_recv, pq_send, pq_recv, fq_send, fq_recv,
     z_send, a_send, b_send, kx_recv,
     wa_send, wa_recv, wb_send, wb_recv, wm_send, wm_recv,
@@ -222,13 +281,22 @@
             "sp", (target * ny + y) * 2 + side,
         )
 
+    def direct(d, target):
+        return jnp.logical_not((target >= deep) & (d == deep - 1) & (deep >= 3))
+
+    def onward(r, way):
+        return remote(
+            kx.at[r], kx.at[r], onward_send.at[way], kx_recv.at[r], "sp",
+            (lax.rem(z + 1, nz) * ny + y) * 2 + side,
+        )
+
     ring_a(far).start()
     if b_hops:
         ring_b(far).start()
     for d in range(1, nz):
         target, copy = column(d)
 
-        @pl.when(needs(z, target))
+        @pl.when(needs(z, target) & direct(d, target))
         def _():
             copy.start()
 
@@ -289,36 +357,84 @@
     peak[2:4] = jnp.full((2, 1, lanes), masked_value, f32)
     acc[2:4] = jnp.zeros((2,) + acc.shape[1:], f32)
 
-    top_row = jnp.where(heavy, z, jnp.maximum(z, other_z - deep))
-    row_n = jnp.where(heavy, deep, top_row + 1)
+    kinds = []
+    for at in list(range(deep)) + [deep]:
+        event_list, first_events, item_list, lent_end = plan(at, nz, ny)
+        event_codes, item_codes = [], []
+        for row, step in event_list:
+            d = (step + 1) // 2
+            spread = step == 0 or not (at >= deep and at - row == deep)
+            along = int((step == 0 or step % 2 == 1) and d < a_hops and spread)
+            back = int(step % 2 == 0 and d < b_hops and spread)
+            event_codes.append(((at - row + nz) * 16 + step) * 4 + along * 2 + back)
+        for row, step, q, pad, need in item_list:
+            item_codes.append((((at - row + nz) * 16 + step) * 4 + q * 2 + pad) * 64 + need)
+        kinds.append((event_codes, item_codes, first_events, lent_end))
+
+    def by_kind(values):
+        chosen = jnp.int32(values[deep])
+        for at in range(deep):
+            if values[at] != values[deep]:
+                chosen = jnp.where(z == at, values[at], chosen)
+        return chosen
+
+    def column_of(index):
+        size = max(len(kind[index]) for kind in kinds)
+        return [by_kind([(kind[index] + [0] * size)[n] for kind in kinds]) for n in range(size)]
+
+    all_events, all_items = column_of(0), column_of(1)
+    events = by_kind([len(kind[0]) for kind in kinds])
+    items = by_kind([len(kind[1]) for kind in kinds])
+    ahead = by_kind([kind[2] for kind in kinds])
+    partner_items = by_kind([kind[3] for kind in kinds])
+
+    def lookup(codes, n):
+        level, codes = 1, list(codes)
+        while len(codes) > 1:
+            odd = lax.rem(lax.div(n, level), 2) == 1
+            codes = [
+                jnp.where(odd, codes[k + 1], codes[k]) if k + 1 < len(codes) else codes[k]
+                for k in range(0, len(codes), 2)
+            ]
+            level *= 2
+        return codes[0]
+
+    def tile_of(place):
+        away, step = lax.div(place, 16) - nz, lax.rem(place, 16)
+        d, odd = lax.div(step + 1, 2), lax.rem(step, 2)
+        source = lax.rem(y + jnp.where(odd == 1, -d, d) * sign + ny, ny)
+        return (z - away) * ny + source, away, step
 
     def event(e):
-        step, at = lax.div(e, row_n), lax.rem(e, row_n)
-        d = lax.div(step + 1, 2)
-        odd = lax.rem(step, 2)
-        source = lax.rem(y + jnp.where(odd == 1, -d, d) * sign + ny, ny)
-        along_a = ((step == 0) | (odd == 1)) & (d < a_hops)
-        along_b = (odd == 0) & (d < b_hops)
-        return (top_row - at) * ny + source, along_a, along_b
+        code = lookup(all_events, e)
+        r, away, step = tile_of(lax.div(code, 4))
+        ways = lax.rem(code, 4)
+        pass_on = (step == 0) & (z + 1 >= deep) & (z + 1 < nz) & (deep >= 3)
+        along_z = jnp.where(
+            pass_on & (away == deep - 2), 1, jnp.where(pass_on & (away == deep - 1), 2, 0)
+        )
+        return r, ways >= 2, lax.rem(ways, 2) == 1, along_z
 
     def arrive(e, carry):
-        r, along_a, along_b = event(e)
-
-        @pl.when(r != far)
+        r, along_a, along_b, along_z = event(e)
+        ring_a(r).wait_recv()
+
+        for way in range(2):
+            @pl.when(along_z == way + 1)
+            def _():
+                onward(r, way).start()
+
+        @pl.when(along_a)
         def _():
-            ring_a(r).wait_recv()
-
-            @pl.when(along_a)
-            def _():
-                ring_a(r).start()
-
-            @pl.when(along_b)
-            def _():
-                ring_b(r).start()
+            ring_a(r).start()
+
+        @pl.when(along_b)
+        def _():
+            ring_b(r).start()
 
         return carry
 
-    lax.fori_loop(0, row_n, arrive, 0)
+    lax.fori_loop(0, ahead, arrive, 0)
 
     def hear_total(d, carry):
         hear(d).wait_recv()
@@ -352,38 +468,16 @@
             here = slice(h * local_rows, (h + 1) * local_rows)
             peak[g, :, here] = peak[g, :, here] + doubled(own_shift, h)
 
-    lent = jnp.where(heavy, 0, other_z - deep + 1)
-    kept = jnp.where(heavy, deep, z + 1)
-    lag = jnp.where(heavy, 0, min(2, ny - 1))
-    per = kept + lent
-    head_items = lag * lent
-    core_items = (ny - lag) * per
-    items = per * ny
-    partner_items = jnp.where(heavy, items, head_items + core_items - kept)
-
     def item(n):
-        in_head = n < head_items
-        in_core = n < head_items + core_items
-        m = jnp.where(in_head, n, jnp.where(in_core, n - head_items, n - head_items - core_items))
-        group = jnp.where(in_head, jnp.maximum(lent, 1), jnp.where(in_core, per, kept))
-        t, j = lax.div(m, group), lax.rem(m, group)
-        borrowed = in_head | (in_core & (j < lent))
-        k = jnp.where(borrowed, j, jnp.where(in_core, j - lent, j))
-        arrived = jnp.where(in_head, t, jnp.where(in_core, t + lag, ny))
-        step = jnp.where(borrowed, arrived, jnp.where(in_core, t, t + ny - lag))
-        row = jnp.where(borrowed, other_z - deep - k, z - k)
-        d = lax.div(step + 1, 2)
-        odd = lax.rem(step, 2)
-        source = lax.rem(y + jnp.where(odd == 1, -d, d) * sign + ny, ny)
-        skip = jnp.logical_not(borrowed) & (row == z) & (source >= y)
-        exact = borrowed | heavy
-        need = jnp.where(
-            exact, arrived * row_n + top_row - row + 1, jnp.minimum(arrived + 1, ny) * row_n
-        )
-        return row * ny + source, jnp.where(borrowed, 1, 0), skip, jnp.maximum(need, row_n)
-
-    def score_stage(n, b):
-        r, q, _, _ = item(n)
+        code = lookup(all_items, n)
+        head = lax.div(code, 64)
+        r, away, _ = tile_of(lax.div(head, 4))
+        q = lax.div(lax.rem(head, 4), 2)
+        skip = (lax.rem(head, 2) == 1) | ((q == 0) & (away == 0) & (r > far))
+        return r, q, jnp.where(skip, 1, 0), lax.rem(code, 64)
+
+    def score_stage(chosen, b):
+        r, q, _, _ = chosen
         ka = kx[r, 0:ka_rows, :].T
 
         def run(g, here):
@@ -393,12 +487,12 @@
 
         return run
 
-    def sum_stage(n, b):
-        r, q, skip, _ = item(n)
+    def sum_stage(chosen, b):
+        r, q, skip, _ = chosen
         va = kx[r, key_cols:, :]
         chip = jnp.where(q == 0, far, partner_far)
         offset = gq[pl.ds(chip, 1), :] - gk[pl.ds(r, 1), :]
-        offset = jnp.where(skip, skipped_value, offset)
+        offset = jnp.where(skip == 1, skipped_value, offset)
 
         def run(g, here, h):
             o = doubled(offset, h)
@@ -414,20 +508,25 @@
 
     tiles = [(g, h, slice(h * local_rows, (h + 1) * local_rows)) for g in range(2) for h in range(heads)]
 
-    @pl.when(jnp.logical_not(heavy))
-    def _():
+    def take_partner_q():
         partner_q.wait_recv()
         forward_q.start()
         forward_q.wait_recv()
 
-    lax.fori_loop(row_n, item(jnp.int32(0))[3], arrive, 0)
-    begin = score_stage(jnp.int32(0), 0)
+    if ny < 8:
+        pl.when(jnp.logical_not(heavy))(take_partner_q)
+    opening = item(jnp.int32(0))
+    lax.fori_loop(ahead, opening[3], arrive, 0)
+    begin = score_stage(opening, 0)
     for g, h, here in tiles:
         begin(g, here)
 
     def trip(i, carry):
         n = 2 * i
-        lax.fori_loop(item(n)[3], item(jnp.minimum(n + 2, items - 1))[3], arrive, 0)
+        if ny >= 8:
+            pl.when(jnp.logical_not(heavy) & (i == 1))(take_partner_q)
+        chosen = carry
+        lax.fori_loop(chosen[0][3], chosen[2][3], arrive, 0)
 
         @pl.when(i == lax.div(items, 4))
         def _():
@@ -445,13 +544,12 @@
                 wo_mate(d).start()
 
         for b in range(2):
-            now = n + b
-            scores = score_stage(jnp.minimum(now + 1, items - 1), 1 - b)
-            sums_now = sum_stage(now, b)
+            scores = score_stage(chosen[b + 1], 1 - b)
+            sums_now = sum_stage(chosen[b], b)
             for g, h, here in tiles:
                 scores(g, here)
                 sums_now(g, here, h)
-        return carry
+        return (chosen[2],) + tuple(item(jnp.minimum(n + k, items - 1)) for k in (3, 4))
 
     def to_mate(q):
         return remote(
@@ -476,7 +574,8 @@
         remote(ret_s, in_s, r_send.at[1], r_recv.at[1], "sp", partner),
     ]
     half_trips = lax.div(partner_items + 1, 2)
-    lax.fori_loop(0, half_trips, trip, 0)
+    carried = (opening,) + tuple(item(jnp.minimum(jnp.int32(k), items - 1)) for k in (1, 2))
+    carried = lax.fori_loop(0, half_trips, trip, carried)
 
     @pl.when(jnp.logical_not(heavy))
     def _():
@@ -493,7 +592,7 @@
         for copy in ret_copies:
             copy.start()
 
-    lax.fori_loop(half_trips, lax.div(items, 2), trip, 0)
+    lax.fori_loop(half_trips, lax.div(items, 2), trip, carried)
     acc[1 - side, PEAK:PEAK + 1, :] = peak[1 - side]
     to_mate(0).start()
     to_mate(0).wait_recv()
@@ -550,12 +649,17 @@
     for d in range(1, nz):
         target, copy = column(d)
 
-        @pl.when(needs(z, target))
+        @pl.when(needs(z, target) & direct(d, target))
         def _():
             copy.wait_send()
 
     def drain(e, carry):
-        r, along_a, along_b = event(e)
+        r, along_a, along_b, along_z = event(e)
+
+        for way in range(2):
+            @pl.when(along_z == way + 1)
+            def _():
+                onward(r, way).wait_send()
 
         @pl.when(along_a)
         def _():
@@ -567,7 +671,10 @@
 
         return carry
 
-    lax.fori_loop(0, row_n * ny, drain, 0)
+    ring_a(far).wait_send()
+    if b_hops:
+        ring_b(far).wait_send()
+    lax.fori_loop(0, events, drain, 0)
     to_mate(0).wait_send()
 
     @pl.when(heavy)
@@ -664,6 +771,7 @@
             dma,
             dma((far_n,)),
             dma((far_n,)),
+            dma((2,)),
             dma,
             dma,
             dma,

time: 81.7 us -> 80.3 us (0.983)
  the two profiles are of different devices: /device:TPU:192 before, /device:TPU:1 now
where the time goes in v3:
time: 80.3 us; the launch traced here: 80.2 us
  Pallas kernels  78.5 us (98%)
  local copies, waits for them, and re-layouts  1.67 us (2%)
    pallas_call x1, Pallas kernels, shards(): pl.pallas_call(functools.partial(kernel, sp, tp, ny, chunks), out_shape=j...  78.5 us
    unnamed x1, local copies, waits for them, and re-layouts  1.67 us

profile of v3, /device:TPU:1, one launch (start us, length us, event | category | flops | bytes accessed | tf_op | source)
XLA Modules:
  0.0 80.2 jit_solution(8781786575157360505)
XLA Ops:
  0.0 78.5 %shard_map.73 = bf16[64,2048]{1,0:T(8,128)(2,1)} custom-call(bf16[64,2048]{1,0:T(8,128)(2,1)} %tokens.1, bf16[2048,256]{1,0:T(8,128)(2,1)} %w_query.1, bf16[64,2048]{1,0:T(8,128)(2,1)} %bitcast.3, bf16[64,2048]{1,0:T(8,128)(2,1)} %bitcast.4, bf16[4,2048]{1,0:T(4,128)(2,1)} %bitcast.5, f32[4]{0:T(128)} %bias_in.1, bf16[256,2048]{1,0:T(8,128)(2,1)} %w_output.1), custom_call_target="tpu_custom_call" | custom-call | tf_op jit(solution)/shard_map/pallas_call | solution.py:733
  78.5 1.7 %copy.9 = bf16[64,2048]{1,0:T(8,128)(2,1)} copy(bf16[64,2048]{1,0:T(8,128)(2,1)} %shard_map.73) | data formatting | bytes 524288
